TPU v7x, 256 devices: a 4x2x16 block of a 4x16x16 slice. The times are simulated.
256 devices in a mesh: grp: 2 (over y), ep: 32 (over z, core), tp: 4 (over x).
Axes of the slice: x: 4, y: 2, z: 16, core: 2. Of those that a mesh axis runs over, the one named last changes fastest.
The devices are a block of a 4x16x16 slice.
Arguments:
- query_vectors: bfloat16 [32768, 2048], P(('grp', 'ep'), 'tp'), parts along dimension 0, may hold values from -6 to 6
- attend_lookup_vectors: bfloat16 [32768, 2048], P(('grp', 'ep'), 'tp'), parts along dimension 0, may hold values from -6 to 6
- attend_content_vectors: bfloat16 [32768, 2048], P(('grp', 'ep'), 'tp'), parts along dimension 0, may hold values from -6 to 6
- forget_speed_dependent: bfloat16 [32768, 2048], P(('grp', 'ep'), 'tp'), parts along dimension 0, may hold values from -3 to 3
- amend_speed_dependent: bfloat16 [32768, 2048], P(('grp', 'ep'), 'tp'), parts along dimension 0, may hold values from -6 to 6
- result_switch_preactivation: bfloat16 [32768, 2048], P(('grp', 'ep'), 'tp'), parts along dimension 0, may hold values from -6 to 6
- feature_forget_baseline: float32 [2048], P('tp'), may hold values from -13 to -3
- amend_speed_baseline: float32 [2048], P('tp'), may hold values from -9 to 3
- sudden_forget_extra: float32 [32768, 32], P(('grp', 'ep'), 'tp'), parts along dimension 0, may hold values from -1 to 0
- group_scaling_factor: float32 [2048], P('tp'), may hold values from 0.1 to 1.9
- result_mapping_matrix: bfloat16 [2048, 2048], P('tp'), may hold values from -0.125 to 0.125
- specialist_tokens_activations: bfloat16 [32768, 2048], P(('grp', 'ep', 'tp')), parts along dimension 0, may hold values from -6 to 6
- specialist_scaling_factor: float32 [2048], replicated, may hold values from 0.1 to 1.9
- selected_specialists: int32 [32768, 2], P(('grp', 'ep', 'tp')), parts along dimension 0, may hold values from 0 to 31, all different within a row; in each aligned block of 128 rows (0 to 127, 128 to 255, ...) at most 12 rows name the same one
- selection_mixing_factors: float32 [32768, 2], P(('grp', 'ep', 'tp')), parts along dimension 0, may hold values from 0.3 to 1.5
- dispatched_switch_matrix: bfloat16 [32, 2048, 1024], P('ep', None, 'tp'), may hold values from -0.125 to 0.125
- dispatched_raising_matrix: bfloat16 [32, 2048, 1024], P('ep', None, 'tp'), may hold values from -0.125 to 0.125
- dispatched_lowering_matrix: bfloat16 [32, 1024, 2048], P('ep', 'tp'), may hold values from -0.1875 to 0.1875
- common_switch_matrix: bfloat16 [2048, 512], P(None, 'tp'), may hold values from -0.125 to 0.125
- common_raising_matrix: bfloat16 [2048, 512], P(None, 'tp'), may hold values from -0.125 to 0.125
- common_lowering_matrix: bfloat16 [512, 2048], P('tp'), may hold values from -0.25 to 0.25
Outputs:
- attend_result_matrix: bfloat16 [32768, 2048], P(('grp', 'ep', 'tp')), parts along dimension 0
- moe_out: bfloat16 [32768, 2048], P(('grp', 'ep', 'tp')), parts along dimension 0
There are 2 independent parts, one for each index of `grp`. A program takes and returns all parts, laid end to end along the dimension named above; an argument that names none is the same for every part. Nothing has to cross between parts.
Inputs may be any that keep to these rules, and one draw needn't show every extreme that they name: `selected_specialists`: each row names 2 different experts. Among the rows of one device no expert is named more than 12 times, and in every draw some device names some expert exactly 12 times.
All inputs are finite; a program needn't handle non-finite values.
Results may differ from a plain program's by a relative error of at most 0.023.
Values may be sent and summed in bfloat16 or wider, within the bound.
No kernel may reach another device: no remote copies, remote signals or barrier semaphores. Data moves between devices by JAX's collectives and lax.ppermute only.
A program may use at most 128 MiB of HBM per device.

v0:
```python
import math

import jax
import jax.numpy as jnp
from jax import lax
from jax.sharding import PartitionSpec as P


def carried_in(shard, axis, combine, identity):
    count, position = (lax.axis_size(axis), lax.axis_index(axis))
    everything = jax.tree.map(
        lambda part, kind: lax.all_gather(part.astype(kind), axis),
        shard,
        (jnp.bfloat16, jnp.bfloat16),
    )
    start = jax.tree.map(
        lambda part, zero: jnp.broadcast_to(jnp.asarray(zero, part.dtype), part.shape),
        shard,
        identity,
    )

    def step(k, before):
        reached = k < position
        new = combine(
            before, jax.tree.map(lambda part, own: part[k].astype(own.dtype), everything, shard)
        )
        return jax.tree.map(lambda a, b: jnp.where(reached, a, b), new, before)

    return lax.fori_loop(0, count, step, start)


def masked_pair(left_side, right_side, pair_mask):
    product = jnp.einsum("shk,jhk->hsj", left_side, right_side)
    return jnp.where(pair_mask[None], product, 0.0)


def block_form(memory, inputs):
    recept_span, decay_span, write_span, value_span, unit_span, erase_span = inputs
    span_len = recept_span.shape[0]
    decay_cum = jnp.cumsum(decay_span, axis=0)
    decay_prev = decay_cum - decay_span
    middle = decay_cum[span_len // 2]
    erase_dir = -unit_span
    left_erase = erase_dir * jnp.exp(decay_prev - middle)
    left_read = recept_span * jnp.exp(decay_cum - middle)
    right_erase = erase_span * jnp.exp(middle - decay_cum)
    right_write = write_span * jnp.exp(middle - decay_cum)
    positions = jnp.arange(span_len)
    strict = positions[:, None] > positions[None, :]
    inclusive = positions[:, None] >= positions[None, :]
    erase_erase = masked_pair(left_erase, right_erase, strict)
    erase_write = masked_pair(left_erase, right_write, strict)
    read_erase = masked_pair(left_read, right_erase, inclusive)
    read_write = masked_pair(left_read, right_write, inclusive)
    value_pad = jnp.concatenate([value_span, jnp.zeros_like(value_span)], axis=2)
    solve_rhs = jnp.einsum("shk,hrk->hsr", erase_dir * jnp.exp(decay_prev), memory)
    solve_rhs = solve_rhs + jnp.einsum("hsj,jhr->hsr", erase_write, value_pad)
    identity = jnp.eye(span_len, dtype=jnp.float32)
    updates = jax.scipy.linalg.solve_triangular(
        identity[None] - erase_erase, solve_rhs, lower=True, unit_diagonal=True
    )
    outputs = jnp.einsum("shk,hrk->hsr", recept_span * jnp.exp(decay_cum), memory)
    outputs = outputs + jnp.einsum("hsj,hjr->hsr", read_erase, updates)
    outputs = outputs + jnp.einsum("hsj,jhr->hsr", read_write, value_pad)
    tail_decay = jnp.exp(decay_cum[-1][None] - decay_cum)
    memory = memory * jnp.exp(decay_cum[-1])[:, None, :]
    memory = memory + jnp.einsum("hjr,jhk->hrk", updates, erase_span * tail_decay)
    memory = memory + jnp.einsum("jhr,jhk->hrk", value_pad, write_span * tail_decay)
    return (memory, outputs)


def chain_pair(earlier_part, later_part):
    joined_map = jnp.einsum("hij,hjk->hik", earlier_part[0], later_part[0])
    joined_add = jnp.einsum("hij,hjk->hik", earlier_part[1], later_part[0]) + later_part[1]
    return (joined_map, joined_add)


def mixer_half(
    query_vectors,
    attend_lookup_vectors,
    attend_content_vectors,
    forget_speed_dependent,
    amend_speed_dependent,
    result_switch_preactivation,
    feature_forget_baseline,
    amend_speed_baseline,
    sudden_forget_extra,
    group_scaling_factor,
):
    tokens, mix_width = query_vectors.shape
    attend_group_total = sudden_forget_extra.shape[1]
    head_size = mix_width // attend_group_total

    def split_among_groups(array_in):
        return array_in.astype(jnp.float32).reshape(tokens, attend_group_total, head_size)

    forget_exponent_log = (
        -jnp.exp(
            feature_forget_baseline.reshape(attend_group_total, head_size)
            + split_among_groups(forget_speed_dependent)
        )
        + sudden_forget_extra[:, :, None]
    )
    learn_rate = jax.nn.sigmoid(
        amend_speed_baseline.reshape(attend_group_total, head_size)
        + split_among_groups(amend_speed_dependent)
    )
    key_heads = split_among_groups(attend_lookup_vectors)
    unit_key = key_heads * lax.rsqrt(jnp.sum(key_heads * key_heads, -1, keepdims=True) + 1e-06)
    span_len = math.gcd(tokens, 64)
    span_count = tokens // span_len

    def by_span(array_in):
        return array_in.reshape(span_count, span_len, attend_group_total, head_size)

    eye_heads = jnp.broadcast_to(
        jnp.eye(head_size, dtype=jnp.float32), (attend_group_total, head_size, head_size)
    )
    zero_heads = jnp.zeros((attend_group_total, head_size, head_size), jnp.float32)
    memory_zero = jnp.concatenate([zero_heads, eye_heads], axis=1)
    memory_end, outputs = lax.scan(
        block_form,
        memory_zero,
        (
            by_span(split_among_groups(query_vectors)),
            by_span(forget_exponent_log),
            by_span(key_heads * learn_rate),
            by_span(split_among_groups(attend_content_vectors)),
            by_span(unit_key),
            by_span(unit_key * learn_rate),
        ),
    )
    carried = memory_end[:, head_size:, :]
    offset = memory_end[:, :head_size, :]
    prefix = carried_in((carried, offset), "ep", chain_pair, (eye_heads, zero_heads))
    start_state = prefix[1]
    flat_out = outputs.transpose(0, 2, 1, 3).reshape(tokens, attend_group_total, 2 * head_size)
    head_out = flat_out[:, :, :head_size] + jnp.einsum(
        "thk,hvk->thv", flat_out[:, :, head_size:], start_state
    )
    head_mean = jnp.mean(head_out, -1, keepdims=True)
    centered = head_out - head_mean
    head_var = jnp.mean(centered * centered, -1, keepdims=True)
    normed = (
        centered
        * lax.rsqrt(head_var + 0.00064)
        * group_scaling_factor.reshape(attend_group_total, head_size)
    )
    mixed_rows = (normed * jax.nn.sigmoid(split_among_groups(result_switch_preactivation))).reshape(
        tokens, mix_width
    )
    return mixed_rows.astype(jnp.bfloat16)


def swiglu_rows(rows, gate_w, up_w):
    gate_vals = jnp.dot(rows, gate_w, preferred_element_type=jnp.float32)
    up_vals = jnp.dot(rows, up_w, preferred_element_type=jnp.float32)
    return (jax.nn.silu(gate_vals) * up_vals).astype(jnp.bfloat16)


def on_device(
    query_vectors,
    attend_lookup_vectors,
    attend_content_vectors,
    forget_speed_dependent,
    amend_speed_dependent,
    result_switch_preactivation,
    feature_forget_baseline,
    amend_speed_baseline,
    sudden_forget_extra,
    group_scaling_factor,
    result_mapping_matrix,
    specialist_tokens_activations,
    specialist_scaling_factor,
    selected_specialists,
    selection_mixing_factors,
    dispatched_switch_matrix,
    dispatched_raising_matrix,
    dispatched_lowering_matrix,
    common_switch_matrix,
    common_raising_matrix,
    common_lowering_matrix,
):
    mixed_rows = mixer_half(
        query_vectors,
        attend_lookup_vectors,
        attend_content_vectors,
        forget_speed_dependent,
        amend_speed_dependent,
        result_switch_preactivation,
        feature_forget_baseline,
        amend_speed_baseline,
        sudden_forget_extra,
        group_scaling_factor,
    )
    floats = specialist_tokens_activations.astype(jnp.float32)
    normed = (
        floats
        * lax.rsqrt(jnp.mean(floats * floats, -1, keepdims=True) + 1e-06)
        * specialist_scaling_factor
    )
    normed = normed.astype(jnp.bfloat16)
    tok_rows, top_count = selected_specialists.shape
    model_width = specialist_tokens_activations.shape[1]
    experts = lax.axis_size("ep")
    tp_size = lax.axis_size("tp")
    capacity = 3 * tok_rows * top_count // (2 * experts)
    flat_ids = selected_specialists.reshape(-1)
    one_hot = (flat_ids[:, None] == jnp.arange(experts, dtype=jnp.int32)[None, :]).astype(jnp.int32)
    slot_rank = jnp.sum((jnp.cumsum(one_hot, axis=0) - 1) * one_hot, axis=1)
    position = flat_ids * capacity + slot_rank
    placing = position[:, None] == jnp.arange(experts * capacity, dtype=jnp.int32)[None, :]
    placing = jnp.sum(
        placing.astype(jnp.bfloat16).reshape(tok_rows, top_count, experts * capacity), axis=1
    )
    outgoing = jnp.einsum("te,td->ed", placing, normed, preferred_element_type=jnp.float32).astype(
        jnp.bfloat16
    )
    gate_w = dispatched_switch_matrix[0]
    up_w = dispatched_raising_matrix[0]
    down_w = dispatched_lowering_matrix[0]
    received = lax.all_to_all(
        outgoing.reshape(experts, capacity, model_width),
        "ep",
        split_axis=0,
        concat_axis=0,
        tiled=True,
    )
    local_rows = experts * capacity
    hidden = swiglu_rows(
        lax.all_gather(received.reshape(local_rows, model_width), "tp", axis=0, tiled=True),
        gate_w,
        up_w,
    )
    summed = lax.psum_scatter(
        jnp.dot(hidden, down_w, preferred_element_type=jnp.float32).astype(jnp.bfloat16),
        "tp",
        scatter_dimension=0,
        tiled=True,
    )
    expert_out = lax.all_to_all(
        summed.reshape(experts, capacity, model_width),
        "ep",
        split_axis=0,
        concat_axis=0,
        tiled=True,
    ).reshape(experts * capacity, model_width)
    picked = jnp.take(expert_out, position, axis=0).astype(jnp.float32)
    routed = jnp.sum(
        (picked * selection_mixing_factors.reshape(-1)[:, None]).reshape(
            tok_rows, top_count, model_width
        ),
        axis=1,
    )
    shared_hidden = swiglu_rows(
        lax.all_gather(normed, "tp", axis=0, tiled=True),
        common_switch_matrix,
        common_raising_matrix,
    )
    mixer_rows = mixed_rows.shape[0] // tp_size
    per_device = mixer_rows + tok_rows
    first_device = jnp.int32(0) // per_device
    blocks = []
    for turn_id in range(per_device * lax.axis_size("tp") // per_device):
        device = first_device + turn_id
        blocks.append(
            jnp.dot(
                lax.dynamic_slice_in_dim(mixed_rows, device * mixer_rows, mixer_rows, 0),
                result_mapping_matrix,
                preferred_element_type=jnp.float32,
            )
        )
        blocks.append(
            jnp.dot(
                lax.dynamic_slice_in_dim(shared_hidden, device * tok_rows, tok_rows, 0),
                common_lowering_matrix,
                preferred_element_type=jnp.float32,
            )
        )
    joined = lax.psum_scatter(
        jnp.concatenate(blocks, axis=0).astype(jnp.bfloat16), "tp", scatter_dimension=0, tiled=True
    ).astype(jnp.float32)
    attend_result_matrix = joined[:mixer_rows]
    shared_sum = joined[mixer_rows:]
    moe_out = (routed + shared_sum).astype(jnp.bfloat16)
    return (attend_result_matrix.astype(jnp.bfloat16), moe_out)


def solution(mesh):
    placed = (
        P(("grp", "ep"), "tp"),
        P(("grp", "ep"), "tp"),
        P(("grp", "ep"), "tp"),
        P(("grp", "ep"), "tp"),
        P(("grp", "ep"), "tp"),
        P(("grp", "ep"), "tp"),
        P("tp"),
        P("tp"),
        P(("grp", "ep"), "tp"),
        P("tp"),
        P("tp", None),
        P(("grp", "ep", "tp"), None),
        P(),
        P(("grp", "ep", "tp"), None),
        P(("grp", "ep", "tp"), None),
        P("ep", None, "tp"),
        P("ep", None, "tp"),
        P("ep", "tp", None),
        P(None, "tp"),
        P(None, "tp"),
        P("tp", None),
    )
    return jax.shard_map(
        on_device,
        mesh=mesh,
        in_specs=placed,
        out_specs=(P(("grp", "ep", "tp"), None), P(("grp", "ep", "tp"), None)),
        check_vma=False,
    )
```

profile of v0, /device:TPU:33, one launch (start us, length us, event | category | flops | bytes accessed | tf_op | source)
XLA Modules:
  0.0 947.2 jit_solution(15160833496766794190)
XLA Ops:
  14.6 3.6 reshape.237
  18.2 25.6 %all-to-all-start = ((bf16[32,12,2048]{2,1,0:T(8,128)(2,1)}), bf16[32,12,2048]{2,1,0:T(8,128)(2,1)}, u32[]{:S(2)}, u32[]{:S(2)}) async-start(bf16[32,12,2048]{2,1,0:T(8,128)(2,1)} %reshape.237), calls=%async_computation.1 | async-start | bytes 4194304 | tf_op jit(solution)/shard_map/all_to_all | solution.py:222
  46.8 3.7 copy.143
  52.6 2.7 reshape.245
  57.3 2.4 reshape.246
  59.9 5.8 fusion.85
  65.7 76.9 %all-to-all-done = bf16[32,12,2048]{2,1,0:T(8,128)(2,1)} async-done(((bf16[32,12,2048]{2,1,0:T(8,128)(2,1)}), bf16[32,12,2048]{2,1,0:T(8,128)(2,1)}, u32[]{:S(2)}, u32[]{:S(2)}) %all-to-all-start) | async-done | bytes 1572896 | tf_op jit(solution)/shard_map/all_to_all | solution.py:222
  142.6 3.6 reshape.238
  146.3 443.8 %while.26 = (s32[]{:T(128)}, f32[8,128,64]{1,2,0:T(8,128)S(1)}, f32[8,8,64,128]{3,1,2,0:T(8,128)}, f32[8,64,8,64]{3,2,1,0:T(8,128)}, f32[8,64,8,64]{3,2,1,0:T(8,...) while((s32[]{:T(128)}, f32[8,128,64]{1,2,0:T(8,128)S(1)}, ...), condition=%wide.region_3.4_spmd, body=%wide.region_1.3_spmd.sunk | while | flops 129265728 | bytes 8965825 | solution.py:121
  147.4 2.3 bitcast_multiply_fusion.9
  150.5 40.0 %custom-call.11 = f32[8,1,64,64]{2,3,1,0:T(8,128)} custom-call(f32[8,1,64,64]{3,2,1,0:T(8,128)S(1)} %fusion.186), custom_call_target="InvertDiagBlocksLowerTriangular" | custom-call | tf_op jit(solution)/shard_map/while/body/eval_jaxpr/jit(_solve_triangular)/vmap()/triangular_solve | solution.py:59
  198.6 1.8 copy_dynamic-update-slice_fusion.2
  202.8 2.3 bitcast_multiply_fusion.9
  206.0 40.0 %custom-call.11 = f32[8,1,64,64]{2,3,1,0:T(8,128)} custom-call(f32[8,1,64,64]{3,2,1,0:T(8,128)S(1)} %fusion.186), custom_call_target="InvertDiagBlocksLowerTriangular" | custom-call | tf_op jit(solution)/shard_map/while/body/eval_jaxpr/jit(_solve_triangular)/vmap()/triangular_solve | solution.py:59
  254.1 1.8 copy_dynamic-update-slice_fusion.2
  258.3 2.3 bitcast_multiply_fusion.9
  261.5 40.0 %custom-call.11 = f32[8,1,64,64]{2,3,1,0:T(8,128)} custom-call(f32[8,1,64,64]{3,2,1,0:T(8,128)S(1)} %fusion.186), custom_call_target="InvertDiagBlocksLowerTriangular" | custom-call | tf_op jit(solution)/shard_map/while/body/eval_jaxpr/jit(_solve_triangular)/vmap()/triangular_solve | solution.py:59
  313.8 2.3 bitcast_multiply_fusion.9
  317.0 40.0 %custom-call.11 = f32[8,1,64,64]{2,3,1,0:T(8,128)} custom-call(f32[8,1,64,64]{3,2,1,0:T(8,128)S(1)} %fusion.186), custom_call_target="InvertDiagBlocksLowerTriangular" | custom-call | tf_op jit(solution)/shard_map/while/body/eval_jaxpr/jit(_solve_triangular)/vmap()/triangular_solve | solution.py:59
  365.0 1.8 copy_dynamic-update-slice_fusion.2
  369.3 2.3 bitcast_multiply_fusion.9
  372.4 40.0 %custom-call.11 = f32[8,1,64,64]{2,3,1,0:T(8,128)} custom-call(f32[8,1,64,64]{3,2,1,0:T(8,128)S(1)} %fusion.186), custom_call_target="InvertDiagBlocksLowerTriangular" | custom-call | tf_op jit(solution)/shard_map/while/body/eval_jaxpr/jit(_solve_triangular)/vmap()/triangular_solve | solution.py:59
  424.7 2.3 bitcast_multiply_fusion.9
  427.9 40.0 %custom-call.11 = f32[8,1,64,64]{2,3,1,0:T(8,128)} custom-call(f32[8,1,64,64]{3,2,1,0:T(8,128)S(1)} %fusion.186), custom_call_target="InvertDiagBlocksLowerTriangular" | custom-call | tf_op jit(solution)/shard_map/while/body/eval_jaxpr/jit(_solve_triangular)/vmap()/triangular_solve | solution.py:59
  480.2 2.3 bitcast_multiply_fusion.9
  483.4 40.0 %custom-call.11 = f32[8,1,64,64]{2,3,1,0:T(8,128)} custom-call(f32[8,1,64,64]{3,2,1,0:T(8,128)S(1)} %fusion.186), custom_call_target="InvertDiagBlocksLowerTriangular" | custom-call | tf_op jit(solution)/shard_map/while/body/eval_jaxpr/jit(_solve_triangular)/vmap()/triangular_solve | solution.py:59
  531.4 1.8 copy_dynamic-update-slice_fusion.2
  535.7 2.3 bitcast_multiply_fusion.9
  538.9 40.0 %custom-call.11 = f32[8,1,64,64]{2,3,1,0:T(8,128)} custom-call(f32[8,1,64,64]{3,2,1,0:T(8,128)S(1)} %fusion.186), custom_call_target="InvertDiagBlocksLowerTriangular" | custom-call | tf_op jit(solution)/shard_map/while/body/eval_jaxpr/jit(_solve_triangular)/vmap()/triangular_solve | solution.py:59
  592.0 2.9 slice.71
  594.9 2.2 copy.171
  597.1 2.3 add_divide_fusion.1
  599.4 2.5 copy.153
  602.0 2.5 fusion.101
  606.0 6.1 fusion.80
  612.0 12.9 %convolution_convert_fusion = bf16[1536,2048]{1,0:T(8,128)(2,1)} fusion(bf16[1536,2048]{1,0:T(8,128)(2,1)} %all-gather.9.cloned.1.call-done, f32[1536,256]{1,0:T(8,128)} %fusion.80, bf16[1,256,2048]{2,1,0:T(8,128)(2,1)} %param.42, bf16[1,2048,256]{2,1,0:T(8,128)(2,1)} %param.41), kind=kOutput, calls=%fused_computation.85 | convolution fusion | flops 3226730496 | bytes 16252928 | tf_op jit(solution)/shard_map/dot_general | solution.py:236
  625.3 32.4 %all-gather.11.cloned.1.call-done = bf16[256,64,64]{2,1,0:T(8,128)(2,1)} async-done(((bf16[8,64,64]{2,1,0:T(8,128)(2,1)}), bf16[256,64,64]{2,1,0:T(8,128)(2,1)}) %all-gather.11.cloned.1.call-update) | async-done | bytes 2097168 | tf_op jit(solution)/shard_map/all_gather | solution.py:12
  657.7 71.4 %all-gather.13.cloned.1.call-done = bf16[256,64,64]{2,1,0:T(8,128)(2,1)} async-done(((bf16[8,64,64]{2,1,0:T(8,128)(2,1)}), bf16[256,64,64]{2,1,0:T(8,128)(2,1)}) %all-gather.13.cloned.1.call-update) | async-done | bytes 2097168 | tf_op jit(solution)/shard_map/all_gather | solution.py:12
  729.1 72.3 %while.27 = (s32[]{:T(128)}, bf16[8,64,64]{1,2,0:T(8,128)(2,1)S(1)}, s32[]{:T(128)}, bf16[32,8,64,64]{3,2,1,0:T(8,128)(2,1)}, bf16[32,8,64,64]{3,2,1,0:T(8,128)(2,1)}, /*index=5*/s32[]{:T(128)}, s32[]{:T(128)}) while((s32[]{:T(128)}, bf16[8,64,64]{1,2,0:T(8,128)(2,1)S(1)}, s32[]{:T(128)}, bf16[32,8,64,64]{3,2,1,0:T(8,128)(2,1)}, ...), condition=%wide.region_5.6_spmd.clone, body=%wide.region_4.5_spmd.clone.sunk | while | flops 4358148 | bytes 985187 | solution.py:29
  801.4 1.9 fusion.100
  813.5 3.6 reshape.239
  817.1 8.9 all-to-all-start.1
  826.6 36.8 %reduce-scatter.3.cloned.1.call-done = bf16[256,2048]{1,0:T(8,128)(2,1)} async-done(((bf16[1024,2048]{1,0:T(8,128)(2,1)}), bf16[256,2048]{1,0:T(8,128)(2,1)}) %reduce-scatter.3.cloned.1.call-update) | async-done | bytes 1048592 | tf_op jit(solution)/shard_map/reduce_scatter | solution.py:280
  863.4 1.9 slice.72
  865.2 59.5 %all-to-all-done.1 = bf16[32,12,2048]{2,1,0:T(8,128)(2,1)} async-done(((bf16[32,12,2048]{2,1,0:T(8,128)(2,1)}), bf16[32,12,2048]{2,1,0:T(8,128)(2,1)}, u32[]{:S(2)}, u32[]{:S(2)}) %all-to-all-start.1) | async-done | bytes 1572896 | tf_op jit(solution)/shard_map/all_to_all | solution.py:241
  924.7 3.7 reshape.240
  928.4 4.0 gather_fusion
  933.9 5.5 multiply_reduce_fusion
  (431 shorter events, 199.9 us)
Async XLA Ops:
  7.2 796.7 %copy-start = (bf16[512,2048]{1,0:T(8,128)(2,1)S(1)}, bf16[512,2048]{1,0:T(8,128)(2,1)}, u32[]{:S(2)}) copy-start(bf16[512,2048]{1,0:T(8,128)(2,1)} %param.35) | copy-start | bytes 6291460
  12.9 5.4 copy-start.5
  18.2 26.5 %copy-start.11 = (bf16[512,512]{1,0:T(8,128)(2,1)S(1)}, bf16[512,512]{1,0:T(8,128)(2,1)}, u32[]{:S(2)}) copy-start(bf16[512,512]{1,0:T(8,128)(2,1)} %param.26) | copy-start | bytes 1572868
  18.2 124.3 %all-to-all-start = ((bf16[32,12,2048]{2,1,0:T(8,128)(2,1)}), bf16[32,12,2048]{2,1,0:T(8,128)(2,1)}, u32[]{:S(2)}, u32[]{:S(2)}) async-start(bf16[32,12,2048]{2,1,0:T(8,128)(2,1)} %reshape.237), calls=%async_computation.1 | async-start | bytes 4194304 | tf_op jit(solution)/shard_map/all_to_all | solution.py:222
  43.9 558.2 %all-gather.7.cloned.1.call-start = ((), (), s32[]{:S(2)}) async-start(), calls=%async_computation.4 | async-start | bytes 2621440 | tf_op jit(solution)/shard_map/all_gather | solution.py:256
  44.6 561.3 %all-gather.9.cloned.1.call-start = ((), (), s32[]{:S(2)}) async-start(), calls=%async_computation.6 | async-start | bytes 7864320 | tf_op jit(solution)/shard_map/all_gather | solution.py:231
  46.8 4.0 copy-start.9
  50.8 4.5 copy-start.13
  52.5 2.9 copy-start.15
  52.6 3.0 copy-start.16
  52.6 3.0 copy-start.10
  146.2 511.4 %all-gather.11.cloned.1.call-start = ((), (), s32[]{:S(2)}) async-start(), calls=%async_computation.8 | async-start | bytes 4325376 | tf_op jit(solution)/shard_map/all_gather | solution.py:12
  149.6 0.6 copy-start.1
  149.6 0.7 copy-start.2
  194.4 7.2 copy-start.3
  205.1 0.6 copy-start.1
  205.1 0.7 copy-start.2
  249.9 7.2 copy-start.3
  260.6 0.6 copy-start.1
  260.6 0.7 copy-start.2
  305.4 7.2 copy-start.3
  316.1 0.6 copy-start.1
  316.1 0.7 copy-start.2
  360.8 7.2 copy-start.3
  371.5 0.6 copy-start.1
  371.6 0.7 copy-start.2
  416.3 7.2 copy-start.3
  427.0 0.6 copy-start.1
  427.0 0.7 copy-start.2
  471.8 7.2 copy-start.3
  482.5 0.7 copy-start.2
  527.2 7.2 copy-start.3
  538.0 0.6 copy-start.1
  538.0 0.7 copy-start.2
  582.7 7.1 copy-start.3
  591.1 138.0 %all-gather.13.cloned.1.call-start = ((), (), s32[]{:S(2)}) async-start(), calls=%async_computation.9 | async-start | bytes 4325376 | tf_op jit(solution)/shard_map/all_gather | solution.py:12
  591.7 221.7 %reduce-scatter.5.cloned.1.call-start = ((), (), s32[]{:S(2)}) async-start(), calls=%async_computation.7 | async-start | bytes 7864320 | tf_op jit(solution)/shard_map/reduce_scatter | solution.py:235
  597.1 4.9 copy-start.17
  602.0 2.5 copy-start.7
  602.0 2.6 copy-start.19
  625.0 238.3 %reduce-scatter.3.cloned.1.call-start = ((), (), s32[]{:S(2)}) async-start(), calls=%async_computation.5 | async-start | bytes 5242880 | tf_op jit(solution)/shard_map/reduce_scatter | solution.py:280
  801.4 2.1 copy-start.6
  803.7 1.4 copy-start.4
  803.7 1.4 copy-start.12
  817.1 8.9 copy-start.14
  817.1 9.3 copy-start.18
  817.1 107.6 %all-to-all-start.1 = ((bf16[32,12,2048]{2,1,0:T(8,128)(2,1)}), bf16[32,12,2048]{2,1,0:T(8,128)(2,1)}, u32[]{:S(2)}, u32[]{:S(2)}) async-start(bf16[32,12,2048]{2,1,0:T(8,128)(2,1)} %reshape.239), calls=%async_computation.3 | async-start | bytes 4194304 | tf_op jit(solution)/shard_map/all_to_all | solution.py:241
  933.9 5.6 copy-start.8
  (1 other events, 0.6 us)
Sparse Core Ops, SparseCore 0:
  47.1 38.1 all-gather.6
  146.4 65.9 all-gather.8
  591.2 66.3 all-gather.10
  659.9 69.0 all-gather.12
  731.5 66.8 reduce-scatter.4
  813.6 49.7 reduce-scatter.2
where the time goes:
time: 951 us; the launch traced here: 947 us
  other arithmetic  366 us (38%)
  waiting for transfers between devices  278 us (29%)
  matrix products  142 us (15%)
  local copies, waits for them, and re-layouts  108 us (11%)
  starting transfers between devices  35.3 us (4%)
  between operations  14.5 us (2%)
    another operation x16, other arithmetic, block_form(): jax.scipy.linalg.solve_triangular(identity[None] - erase_erase, solve_rhs...  320 us
    all_gather x2, waiting for transfers between devices, carried_in(): lax.all_gather(part.astype(kind), axis)  104 us
    all_to_all x1, waiting for transfers between devices, on_device(): lax.all_to_all(outgoing.reshape(experts, capacity, model_width), 'ep', sp...  76.9 us
    all_to_all x1, waiting for transfers between devices, on_device(): lax.all_to_all(summed.reshape(experts, capacity, model_width), 'ep', spli...  59.5 us
    dot_general x32, matrix products, chain_pair(): jnp.einsum('hij,hjk->hik', earlier_part[1], later_part[0]) + later_part[1]  37 us
    reduce_scatter x1, waiting for transfers between devices, on_device(): lax.psum_scatter(jnp.concatenate(blocks, axis=0).astype(jnp.bfloat16), 't...  36.8 us
    dynamic_slice x64, local copies, waits for them, and re-layouts, step(): part[k].astype(own.dtype)  33.5 us
    all_to_all x1, starting transfers between devices, on_device(): lax.all_to_all(outgoing.reshape(experts, capacity, model_width), 'ep', sp...  25.6 us
  transfers between devices with their start and end apart: 8, of which 5 were waited for; matrix products, arithmetic and copies ran while one was open for 62% of the time, Pallas kernels for 0%

commit v1 on v0

v1 whole, which is shorter than its diff:
```python
import jax
import jax.numpy as jnp
from jax import lax
from jax.experimental import pallas as pl
from jax.experimental.pallas import tpu as pltpu
from jax.sharding import PartitionSpec as P


F32 = jnp.float32
BF16 = jnp.bfloat16
SPAN = 64
VMEM_LIMIT = 56 * 1024 * 1024


def mm(a, b):
    return lax.dot_general(a, b, (((1,), (0,)), ((), ())), preferred_element_type=F32)


def mm_nt(a, b):
    return lax.dot_general(a, b, (((1,), (1,)), ((), ())), preferred_element_type=F32)


def mm_tn(a, b):
    return lax.dot_general(a, b, (((0,), (0,)), ((), ())), preferred_element_type=F32)


def iota(shape, dim):
    return lax.broadcasted_iota(jnp.int32, shape, dim)


def split_two(x):
    hi = x.astype(BF16)
    lo = (x - hi.astype(F32)).astype(BF16)
    return hi, lo


def sigmoid(x):
    return 1.0 / (1.0 + jnp.exp(-x))


def mixer_local(q_ref, k_ref, v_ref, f_ref, a_ref, x_ref, fb_ref, ab_ref, out_ref, q2_ref, ex_ref):
    tokens, width = q_ref.shape
    half = width // 2
    spans = tokens // SPAN
    parts = ex_ref.shape[0] // 2
    rows_per = half // parts
    pair = pl.program_id(0)
    lane = iota((SPAN, width), 1)
    row = iota((SPAN, width), 0)
    first = lane < half
    col = lane % half
    strict = row > col
    inclusive = row >= col
    eye = (row == col).astype(F32)
    tril = (iota((SPAN, SPAN), 0) >= iota((SPAN, SPAN), 1)).astype(BF16)
    ones_bd = ((iota((2 * width, width), 0) % width) // half == iota((2 * width, width), 1) // half).astype(BF16)
    levels = []
    size = 1
    while size < SPAN:
        levels.append(
            (row // (2 * size) == col // (2 * size)) & (row % (2 * size) >= size) & (col % (2 * size) < size)
        )
        size *= 2

    def bd(x):
        zero = jnp.zeros_like(x)
        return jnp.concatenate([jnp.where(first, x, zero), jnp.where(first, zero, x)], axis=0)

    heads = x_ref.shape[1]
    head_lane = iota((SPAN, heads), 1)
    fb = fb_ref[...]
    ab = ab_ref[...]

    def prepare(c):
        rows = pl.ds(c * SPAN, SPAN)
        extra = x_ref[rows, :]
        extra_a = jnp.sum(jnp.where(head_lane == 2 * pair, extra, 0.0), axis=1, keepdims=True)
        extra_b = jnp.sum(jnp.where(head_lane == 2 * pair + 1, extra, 0.0), axis=1, keepdims=True)
        decay = jnp.where(first, extra_a, extra_b) - jnp.exp(fb + f_ref[rows, :].astype(F32))
        hi = decay.astype(BF16)
        rest = decay - hi.astype(F32)
        mid = rest.astype(BF16)
        low = (rest - mid.astype(F32)).astype(BF16)
        sums = mm(tril, jnp.concatenate([hi, mid, low], axis=1))
        cum = sums[:, :width] + sums[:, width : 2 * width] + sums[:, 2 * width :]
        key = k_ref[rows, :].astype(F32)
        sq_hi, sq_lo = split_two(key * key)
        total = mm(jnp.concatenate([sq_hi, sq_lo], axis=1), ones_bd) + 1e-06
        inv = lax.rsqrt(total)
        unit = key * inv
        erase = unit * sigmoid(ab + a_ref[rows, :].astype(F32))
        scaled_value = v_ref[rows, :].astype(F32) * (total * inv)
        center = cum[SPAN // 2 : SPAN // 2 + 1, :]
        last = cum[SPAN - 1 : SPAN, :]
        left_erase = -unit * jnp.exp(cum - decay - center)
        left_read = q_ref[rows, :].astype(F32) * jnp.exp(cum - center)
        right = erase * jnp.exp(center - cum)
        pairs = mm_nt(jnp.concatenate([left_erase, left_read], axis=0).astype(BF16), bd(right.astype(BF16)))
        lower = jnp.where(strict, pairs[:SPAN], 0.0)
        read = jnp.where(inclusive, pairs[SPAN:], 0.0).astype(BF16)
        to_start = jnp.exp(center)
        rhs = jnp.concatenate(
            [bd(scaled_value.astype(BF16)), bd((left_erase * to_start).astype(BF16))], axis=1
        )
        read_start = left_read * to_start
        tail = (right * jnp.exp(last - center)).astype(BF16)
        return lower, read, rhs, read_start, tail, jnp.exp(last)

    state = jnp.concatenate([jnp.zeros((SPAN, width), F32), eye], axis=0)
    group = min(4, spans)
    for start in range(0, spans, group):
        prepared = [prepare(c) for c in range(start, start + group)]
        inverse = [eye + jnp.where(levels[0], p[0], 0.0) for p in prepared]
        for level in levels[1:]:
            packed = [x.astype(BF16) for x in inverse]
            step = [
                mm(x, bd(jnp.where(level, p[0], 0.0).astype(BF16))).astype(BF16)
                for x, p in zip(packed, prepared)
            ]
            inverse = [x + mm(y, bd(xb)) for x, y, xb in zip(inverse, step, packed)]
        solved = [mm(x.astype(BF16), p[2]).astype(BF16) for x, p in zip(inverse, prepared)]
        outs = [
            mm(p[1], jnp.concatenate([bd(u[:, :width]), bd(u[:, width:])], axis=1))
            for u, p in zip(solved, prepared)
        ]
        grams = [mm_tn(u, p[4]) for u, p in zip(solved, prepared)]
        for j in range(group):
            rows = pl.ds((start + j) * SPAN, SPAN)
            out, gram, prep = outs[j], grams[j], prepared[j]
            reads = (out[:, width:] + prep[3]).astype(BF16)
            state_b = state.astype(BF16)
            both = mm_nt(reads, jnp.concatenate([bd(state_b[:SPAN]), bd(state_b[SPAN:])], axis=0))
            out_ref[rows, :] = out[:, :width] + both[:, :width]
            q2_ref[rows, :] = both[:, width:].astype(BF16)
            add = jnp.where(first, gram[:SPAN], gram[SPAN : 2 * SPAN])
            trans = jnp.concatenate(
                [
                    jnp.where(first, gram[2 * SPAN : 3 * SPAN], 0.0),
                    jnp.where(first, 0.0, gram[3 * SPAN :]),
                ],
                axis=0,
            ).astype(BF16)
            state = state * prep[5] + mm(state_b, trans)
            state = jnp.concatenate([state[:SPAN] + add, state[SPAN:]], axis=0)
    offset = state[:SPAN]
    carry = state[SPAN:]
    offset_r = pltpu.roll(offset, half, 1)
    carry_r = pltpu.roll(carry, half, 1)
    h2 = SPAN // 2
    first_h = first[:h2]
    carry_a = jnp.where(first_h, carry[:h2], carry_r[h2:]).astype(BF16)
    carry_b = jnp.where(first_h, carry_r[:h2], carry[h2:]).astype(BF16)
    for head, (carried, added) in enumerate(((carry_a, offset), (carry_b, offset_r))):
        for part in range(parts):
            ex_ref[head * parts + part, 0:h2, :] = carried
            ex_ref[head * parts + part, h2 : h2 + rows_per, :] = added[
                part * rows_per : (part + 1) * rows_per
            ].astype(BF16)


def run_mixer_local(q, k, v, f, a, extra, fb, ab, holders):
    tokens, width = q.shape
    heads = extra.shape[1]
    head_size = width // heads
    pairs = heads // 2
    parts = holders // heads
    wide = 2 * head_size
    rows_per = head_size // parts
    ex_rows = head_size // 2 + rows_per
    spec = pl.BlockSpec((tokens, wide), lambda i: (0, i))
    vec = pl.BlockSpec((1, wide), lambda i: (0, i))
    return pl.pallas_call(
        mixer_local,
        grid=(pairs,),
        in_specs=[spec] * 5 + [pl.BlockSpec((tokens, heads), lambda i: (0, 0)), vec, vec],
        out_specs=[spec, spec, pl.BlockSpec((2 * parts, ex_rows, wide), lambda i: (i, 0, 0))],
        out_shape=[
            jax.ShapeDtypeStruct((tokens, width), F32),
            jax.ShapeDtypeStruct((tokens, width), BF16),
            jax.ShapeDtypeStruct((holders, ex_rows, wide), BF16),
        ],
        compiler_params=pltpu.CompilerParams(
            dimension_semantics=("arbitrary",), vmem_limit_bytes=VMEM_LIMIT
        ),
        cost_estimate=pl.CostEstimate(
            flops=40_000_000_000, transcendentals=2_000_000, bytes_accessed=5_000_000
        ),
        name="mixer_local",
    )(q, k, v, f, a, extra, fb.reshape(1, -1), ab.reshape(1, -1))


def chain_kernel(r_ref, o_ref):
    count, ex_rows, wide = r_ref.shape
    half = wide // 2
    h2 = half // 2
    rows_per = ex_rows - h2
    state = jnp.zeros((rows_per, half), F32)
    for d in range(count):
        block = r_ref[d]
        carried = jnp.concatenate([block[:h2, :half], block[:h2, half:]], axis=0)
        added = block[h2:, :half].astype(F32)
        state_b = state.astype(BF16)
        o_ref[d] = jnp.concatenate([state_b, state_b], axis=1)
        state = mm(state_b, carried) + added


def run_chain(received):
    count, ex_rows, wide = received.shape
    rows_per = ex_rows - wide // 4
    return pl.pallas_call(
        chain_kernel,
        out_shape=jax.ShapeDtypeStruct((count, rows_per, wide), BF16),
        cost_estimate=pl.CostEstimate(
            flops=3_000_000_000, transcendentals=0, bytes_accessed=600_000
        ),
        name="chain",
    )(received)


def mixer_final(me_ref, o_ref, q2_ref, s_ref, g_ref, gain_ref, w_ref, out_ref):
    width = o_ref.shape[1]
    wide = s_ref.shape[1]
    half = wide // 2
    pairs = width // wide
    first = iota((half, wide), 1) < half
    ones_bd = ((iota((2 * wide, wide), 0) % wide) // half == iota((2 * wide, wide), 1) // half).astype(BF16)

    def head_mean(x):
        hi, lo = split_two(x)
        return mm(jnp.concatenate([hi, lo], axis=1), ones_bd) * (1.0 / half)

    pieces = []
    for p in range(pairs):
        cols = slice(p * wide, (p + 1) * wide)
        state_a = s_ref[2 * p * half : (2 * p + 1) * half, :]
        state_b = s_ref[(2 * p + 1) * half : (2 * p + 2) * half, :]
        zero = jnp.zeros_like(state_a)
        both = jnp.concatenate([jnp.where(first, state_a, zero), jnp.where(first, zero, state_b)], axis=0)
        head_out = o_ref[:, cols] + mm_nt(q2_ref[:, cols], both)
        centered = head_out - head_mean(head_out)
        var = head_mean(centered * centered)
        gate = sigmoid(g_ref[:, cols].astype(F32))
        pieces.append((centered * lax.rsqrt(var + 0.00064) * gain_ref[:, cols] * gate).astype(BF16))
    mixed = jnp.concatenate(pieces, axis=1)
    out_ref[0] = mm(mixed, w_ref[...]).astype(BF16)


def run_mixer_final(me, out_local, q2, starts, at, wide, gate, gain, mapping, blocks):
    tokens, width = out_local.shape
    model = mapping.shape[1]
    rows = tokens // blocks

    def turned(i, me_ref):
        return ((me_ref[0] + i) % blocks, 0)

    spec = pl.BlockSpec((rows, width), turned)
    return pl.pallas_call(
        mixer_final,
        grid_spec=pltpu.PrefetchScalarGridSpec(
            num_scalar_prefetch=1,
            grid=(blocks,),
            in_specs=[
                spec,
                spec,
                pl.BlockSpec((starts.shape[0], wide), lambda i, me_ref: (0, at)),
                spec,
                pl.BlockSpec((1, width), lambda i, me_ref: (0, 0)),
                pl.BlockSpec((width, model), lambda i, me_ref: (0, 0)),
            ],
            out_specs=pl.BlockSpec((1, rows, model), lambda i, me_ref: (i, 0, 0)),
        ),
        out_shape=jax.ShapeDtypeStruct((blocks, rows, model), BF16),
        compiler_params=grid_params(),
        cost_estimate=pl.CostEstimate(
            flops=6_000_000_000, transcendentals=1_000_000, bytes_accessed=8_000_000
        ),
        name="mixer_final",
    )(me, out_local, q2, starts, gate, gain.reshape(1, -1), mapping)


def tail_pick(size, slot_rows, cap, third):
    r = iota((size, size), 0)
    c = iota((size, size), 1)
    s = r % slot_rows
    return (
        (r // slot_rows == c // slot_rows) & (s < cap) & (c % slot_rows == cap + s // 3) & (s % 3 == third)
    ).astype(BF16)


def dispatch_kernel(slot_rows, cap, t_ref, scale_ref, sel_ref, normed_ref, out_ref, pos_ref):
    rows, model = t_ref.shape
    total = out_ref.shape[0]
    main = out_ref.shape[1]
    third = main // 3
    experts = total // slot_rows
    floats = t_ref[...].astype(F32)
    mean = jnp.mean(floats * floats, axis=1, keepdims=True)
    normed = (floats * lax.rsqrt(mean + 1e-06) * scale_ref[...]).astype(BF16)
    wide = normed_ref.shape[1]
    for c in range(model // wide):
        normed_ref[c * rows : (c + 1) * rows, :] = normed[:, c * wide : (c + 1) * wide]
    ids = [sel_ref[:, 0:1], sel_ref[:, 1:2]]
    expert = iota((rows, experts), 1)
    hot = [(i == expert).astype(F32) for i in ids]
    strict = (iota((rows, rows), 0) > iota((rows, rows), 1)).astype(BF16)
    before = mm(strict, (hot[0] + hot[1]).astype(BF16))
    slots = [jnp.sum(h * before, axis=1, keepdims=True).astype(jnp.int32) for h in hot]
    place = iota((rows, total), 1)
    pos = [i * slot_rows + s for i, s in zip(ids, slots)]
    tail = [i * slot_rows + cap + s // 3 for i, s in zip(ids, slots)]
    which = [s % 3 for s in slots]
    pos_ref[...] = jnp.concatenate(pos, axis=1)
    main_hot = ((place == pos[0]) | (place == pos[1])).astype(BF16)
    for b in range(3):
        tail_hot = (
            ((place == tail[0]) & (which[0] == b)) | ((place == tail[1]) & (which[1] == b))
        ).astype(BF16)
        hot2 = jnp.concatenate([main_hot, tail_hot], axis=0)
        data = jnp.concatenate([normed[:, b * third : (b + 1) * third], normed[:, main:]], axis=0)
        out_ref[:, b * third : (b + 1) * third] = mm_tn(hot2, data).astype(BF16)


def hidden_kernel(slot_rows, cap, r_ref, g_ref, u_ref, h_ref, tail_ref):
    total, main = r_ref.shape
    third = main // 3
    size = min(256, total)

    @pl.when(pl.program_id(0) == 0)
    def _():
        for start in range(0, total, size):
            acc = jnp.zeros((size, third), F32)
            for b in range(3):
                acc = acc + mm(
                    tail_pick(size, slot_rows, cap, b), r_ref[start : start + size, b * third : (b + 1) * third]
                )
            tail_ref[start : start + size, :] = acc.astype(BF16)

    x = r_ref[...]
    t = tail_ref[...]
    gate = mm(x, g_ref[0, :main, :]) + mm(t, g_ref[0, main:, :])
    up = mm(x, u_ref[0, :main, :]) + mm(t, u_ref[0, main:, :])
    h_ref[...] = (gate * sigmoid(gate) * up).astype(BF16)


def lower_kernel(slot_rows, cap, h_ref, d_ref, t_ref, *refs):
    *extra, o_ref, tail_ref = refs
    total = h_ref.shape[0]
    third = d_ref.shape[2]
    size = min(256, total)
    b = pl.program_id(0)

    @pl.when(b == 0)
    def _():
        tail_ref[...] = mm(h_ref[...], t_ref[...].reshape(-1, third)).astype(BF16)
        for e_ref in extra:
            o_ref[:, 3 * third :] = e_ref[...]

    y = mm(h_ref[...], d_ref[...].reshape(-1, third))
    for start in range(0, total, size):
        moved = mm_tn(tail_pick(size, slot_rows, cap, b), tail_ref[start : start + size, :])
        slot = iota((size, third), 0) % slot_rows
        o_ref[start : start + size, pl.ds(pl.multiple_of(b * third, 128), third)] = jnp.where(
            slot < cap, y[start : start + size], moved
        ).astype(BF16)


def shared_kernel(me_ref, x_ref, g_ref, u_ref, d_ref, o_ref):
    rows = o_ref.shape[1]
    wide = x_ref.shape[2]
    gate = jnp.zeros((rows, g_ref.shape[1]), F32)
    up = jnp.zeros((rows, g_ref.shape[1]), F32)
    for c in range(x_ref.shape[1] // rows):
        x = x_ref[0, c * rows : (c + 1) * rows, :]
        gate = gate + mm(x, g_ref[c * wide : (c + 1) * wide, :])
        up = up + mm(x, u_ref[c * wide : (c + 1) * wide, :])
    hidden = (gate * sigmoid(gate) * up).astype(BF16)
    o_ref[0] = mm(hidden, d_ref[...]).astype(BF16)


def combine_kernel(slot_rows, cap, za_ref, zb_ref, pos_ref, mix_ref, s0_ref, s1_ref, s2_ref, s3_ref, o_ref):
    total, main = zb_ref.shape
    rows = pos_ref.shape[0]
    third = main // 3
    place = iota((rows, total), 1)
    pos = [pos_ref[:, 0:1], pos_ref[:, 1:2]]
    mix = [mix_ref[:, 0:1], mix_ref[:, 1:2]]
    slots = [p % slot_rows for p in pos]
    tail = [p - s + cap + s // 3 for p, s in zip(pos, slots)]
    which = [s % 3 for s in slots]
    weights = jnp.where(place == pos[0], mix[0], 0.0) + jnp.where(place == pos[1], mix[1], 0.0)
    w_hi, w_lo = split_two(weights)
    tails = []
    for b in range(3):
        tails.append(
            split_two(
                jnp.where((place == tail[0]) & (which[0] == b), mix[0], 0.0)
                + jnp.where((place == tail[1]) & (which[1] == b), mix[1], 0.0)
            )
        )

    def shared(cols):
        acc = s0_ref[:, cols].astype(F32)
        for other in (s1_ref, s2_ref, s3_ref):
            acc = acc + other[:, cols].astype(F32)
        return acc

    for half, z_ref in enumerate((za_ref, zb_ref)):
        base = half * (main + third)
        tail_sum = jnp.zeros((rows, third), F32)
        for b in range(3):
            cols = slice(base + b * third, base + (b + 1) * third)
            z = z_ref[:, b * third : (b + 1) * third]
            o_ref[:, cols] = (mm(w_hi, z) + mm(w_lo, z) + shared(cols)).astype(BF16)
            tail_sum = tail_sum + mm(tails[b][0], z) + mm(tails[b][1], z)
        cols = slice(base + main, base + main + third)
        o_ref[:, cols] = (tail_sum + shared(cols)).astype(BF16)


def bind(kernel, *static):
    def body(*refs):
        kernel(*static, *refs)

    body.__name__ = kernel.__name__
    return body


def params():
    return pltpu.CompilerParams(vmem_limit_bytes=VMEM_LIMIT)


def grid_params():
    return pltpu.CompilerParams(dimension_semantics=("arbitrary",), vmem_limit_bytes=VMEM_LIMIT)


def turn_exchange(x, axis):
    count = x.shape[0]
    out = [x[0]]
    for d in range(1, count):
        out.append(lax.ppermute(x[d], axis, [(i, (i + d) % count) for i in range(count)]))
    return out


def exchange(x, axis):
    return lax.all_to_all(x, axis, split_axis=0, concat_axis=0, tiled=True)


def on_device(
    query_vectors,
    attend_lookup_vectors,
    attend_content_vectors,
    forget_speed_dependent,
    amend_speed_dependent,
    result_switch_preactivation,
    feature_forget_baseline,
    amend_speed_baseline,
    sudden_forget_extra,
    group_scaling_factor,
    result_mapping_matrix,
    specialist_tokens_activations,
    specialist_scaling_factor,
    selected_specialists,
    selection_mixing_factors,
    dispatched_switch_matrix,
    dispatched_raising_matrix,
    dispatched_lowering_matrix,
    common_switch_matrix,
    common_raising_matrix,
    common_lowering_matrix,
):
    tok_rows, top_count = selected_specialists.shape
    model = specialist_tokens_activations.shape[1]
    experts = lax.axis_size("ep")
    tp_size = lax.axis_size("tp")
    cap = 3 * tok_rows * top_count // (2 * experts)
    slot_rows = cap * 4 // 3
    main = model * 3 // 4
    third = model // 4
    total = experts * slot_rows

    ff = dispatched_switch_matrix.shape[2]
    half_model = model // 2
    half_main = main // 2
    half_third = third // 2
    low_blocks = half_model // ff

    def stacked(x):
        return x.reshape(ff, low_blocks, ff).transpose(1, 0, 2).reshape(low_blocks * ff, ff)

    lowering = dispatched_lowering_matrix[0]
    early = lax.all_gather(
        jnp.concatenate(
            [
                dispatched_switch_matrix[0],
                dispatched_raising_matrix[0],
                stacked(lowering[:, :half_model]),
            ],
            axis=0,
        ),
        "tp",
    )

    normed, outgoing, positions = pl.pallas_call(
        bind(dispatch_kernel, slot_rows, cap),
        out_shape=[
            jax.ShapeDtypeStruct((tok_rows * model // ff, ff), BF16),
            jax.ShapeDtypeStruct((total, main), BF16),
            jax.ShapeDtypeStruct((tok_rows, top_count), jnp.int32),
        ],
        compiler_params=params(),
        name="dispatch",
    )(specialist_tokens_activations, specialist_scaling_factor.reshape(1, -1), selected_specialists)

    late = lax.all_gather(
        jnp.concatenate([stacked(lowering[:, half_model:]), normed], axis=0), "tp"
    )

    received = exchange(outgoing.reshape(experts, slot_rows, main), "ep").reshape(total, main)

    out_local, q2, outgoing_state = run_mixer_local(
        query_vectors,
        attend_lookup_vectors,
        attend_content_vectors,
        forget_speed_dependent,
        amend_speed_dependent,
        sudden_forget_extra,
        feature_forget_baseline,
        amend_speed_baseline,
        experts,
    )
    states = exchange(outgoing_state, "ep")
    chained = run_chain(states)
    chained = chained.reshape(-1, chained.shape[2])
    wide = chained.shape[1]

    hidden = pl.pallas_call(
        bind(hidden_kernel, slot_rows, cap),
        grid=(tp_size,),
        in_specs=[
            pl.BlockSpec((total, main), lambda i: (0, 0)),
            pl.BlockSpec((1, model, ff), lambda i: (i, 0, 0)),
            pl.BlockSpec((1, model, ff), lambda i: (i, 1, 0)),
        ],
        out_specs=pl.BlockSpec((total, ff), lambda i: (0, i)),
        out_shape=jax.ShapeDtypeStruct((total, ff * tp_size), BF16),
        scratch_shapes=[pltpu.VMEM((total, third), BF16)],
        compiler_params=grid_params(),
        name="hidden",
    )(received, early, early)

    def lower(weights, base, *extra):
        out_width = half_main + sum(e.shape[1] for e in extra)
        return pl.pallas_call(
            bind(lower_kernel, slot_rows, cap),
            grid=(3,),
            in_specs=[
                pl.BlockSpec((total, ff * tp_size), lambda i: (0, 0)),
                pl.BlockSpec((tp_size, ff, half_third), lambda i: (0, base + i, 0)),
                pl.BlockSpec((tp_size, ff, half_third), lambda i: (0, base + 3, 0)),
            ]
            + [pl.BlockSpec(e.shape, lambda i: (0, 0)) for e in extra],
            out_specs=pl.BlockSpec((total, out_width), lambda i: (0, 0)),
            out_shape=jax.ShapeDtypeStruct((total, out_width), BF16),
            scratch_shapes=[pltpu.VMEM((total, half_third), BF16)],
            compiler_params=grid_params(),
            name="lower",
        )(hidden, weights, weights, *extra)

    def send_back(x):
        return exchange(x.reshape(experts, slot_rows, x.shape[1]), "ep").reshape(x.shape)

    first_half = lower(early, 2 * model // ff, chained)
    first_back = send_back(first_half)
    second_half = lower(late, 0)
    second_back = send_back(second_half)

    me = lax.axis_index("tp").astype(jnp.int32).reshape(1)
    sff = common_switch_matrix.shape[1]
    shared_part = pl.pallas_call(
        shared_kernel,
        grid_spec=pltpu.PrefetchScalarGridSpec(
            num_scalar_prefetch=1,
            grid=(tp_size,),
            in_specs=[
                pl.BlockSpec(
                    (1, tok_rows * model // ff, ff), lambda i, me_ref: ((me_ref[0] + i) % tp_size, 1, 0)
                ),
                pl.BlockSpec((model, sff), lambda i, me_ref: (0, 0)),
                pl.BlockSpec((model, sff), lambda i, me_ref: (0, 0)),
                pl.BlockSpec((sff, model), lambda i, me_ref: (0, 0)),
            ],
            out_specs=pl.BlockSpec((1, tok_rows, model), lambda i, me_ref: (i, 0, 0)),
        ),
        out_shape=jax.ShapeDtypeStruct((tp_size, tok_rows, model), BF16),
        compiler_params=grid_params(),
        name="shared",
    )(me, late, common_switch_matrix, common_raising_matrix, common_lowering_matrix)
    shared_blocks = turn_exchange(shared_part, "tp")

    mixed_part = run_mixer_final(
        me,
        out_local,
        q2,
        first_back,
        half_main // wide,
        wide,
        result_switch_preactivation,
        group_scaling_factor,
        result_mapping_matrix,
        tp_size,
    )
    mixed_blocks = turn_exchange(mixed_part, "tp")
    mixed_sum = mixed_blocks[0].astype(F32)
    for block in mixed_blocks[1:]:
        mixed_sum = mixed_sum + block.astype(F32)
    attend_result_matrix = mixed_sum.astype(BF16)
    moe_out = pl.pallas_call(
        bind(combine_kernel, slot_rows, cap),
        out_shape=jax.ShapeDtypeStruct((tok_rows, model), BF16),
        compiler_params=params(),
        name="combine",
    )(first_back, second_back, positions, selection_mixing_factors, *shared_blocks)
    return (attend_result_matrix, moe_out)


def solution(mesh):
    by_rows = P(("grp", "ep"), "tp")
    by_device = P(("grp", "ep", "tp"), None)
    placed = (
        by_rows,
        by_rows,
        by_rows,
        by_rows,
        by_rows,
        by_rows,
        P("tp"),
        P("tp"),
        by_rows,
        P("tp"),
        P("tp", None),
        by_device,
        P(),
        by_device,
        by_device,
        P("ep", None, "tp"),
        P("ep", None, "tp"),
        P("ep", "tp", None),
        P(None, "tp"),
        P(None, "tp"),
        P("tp", None),
    )
    return jax.shard_map(
        on_device, mesh=mesh, in_specs=placed, out_specs=(by_device, by_device), check_vma=False
    )
```

time: 951 us -> 317 us (0.33)
  other arithmetic: 366 us -> 6.21 us
  matrix products: 142 us -> 0 us
  waiting for transfers between devices: 278 us -> 164 us
  local copies, waits for them, and re-layouts: 108 us -> 12.2 us
  Pallas kernels: 0 us -> 70.9 us
  starting transfers between devices: 35.3 us -> 48.3 us
    another operation x26 -> x0, other arithmetic: 329 us -> none  [the longest x16 320 us: block_form(): jax.scipy.linalg.solve_triangular(identity[None] - erase_erase, solve_rhs...]
    dot_general x110 -> x0, matrix products: 130 us -> none  [the longest x32 37 us: chain_pair(): jnp.einsum('hij,hjk->hik', earlier_part[1], later_part[0]) + later_part[1]]
    all_gather x4 -> x2, waiting for transfers between devices: 104 us -> 0.02 us  [the longest x1 0.02 us: on_device(): lax.all_gather(jnp.concatenate([stacked(lowering[:, half_model:]), normed...]
    pallas_call x0 -> x9, Pallas kernels: none -> 70.9 us  [the longest x1 24.9 us: run_mixer_local(): pl.pallas_call(mixer_local, grid=(pairs,), in_specs=[spec] * 5 + [pl.Bloc...]
    dynamic_slice x81 -> x0, local copies, waits for them, and re-layouts: 41.2 us -> none  [the longest x64 33.5 us: step(): part[k].astype(own.dtype)]
    reduce_scatter x2 -> x0, waiting for transfers between devices: 36.8 us -> none  [the longest x1 36.8 us: on_device(): lax.psum_scatter(jnp.concatenate(blocks, axis=0).astype(jnp.bfloat16), 't...]
    reshape x9 -> x2, local copies, waits for them, and re-layouts: 24.7 us -> 0.41 us  [stacked(): x.reshape(ff, low_blocks, ff).transpose(1, 0, 2)]
    mul x10 -> x0, other arithmetic: 23.9 us -> none  [the longest x8 18.1 us: block_form(): erase_span * tail_decay]
  transfers between devices with their start and end apart: 8 -> 12, of which waited for: 5 -> 7; matrix products, arithmetic and copies ran while one was open for 62% -> 3% of each run, Pallas kernels for 0% -> 22%
where the time goes in v1:
time: 317 us; the launch traced here: 316 us
  waiting for transfers between devices  164 us (52%)
  Pallas kernels  70.9 us (22%)
  starting transfers between devices  48.3 us (15%)
  between operations  14.2 us (4%)
  local copies, waits for them, and re-layouts  12.2 us (4%)
  other arithmetic  6.21 us (2%)
    all_to_all x4, waiting for transfers between devices, exchange(): return lax.all_to_all(x, axis, split_axis=0, concat_axis=0, tiled=True)  148 us
    all_to_all x4, starting transfers between devices, exchange(): return lax.all_to_all(x, axis, split_axis=0, concat_axis=0, tiled=True)  40.2 us
    pallas_call x1, Pallas kernels, run_mixer_local(): pl.pallas_call(mixer_local, grid=(pairs,), in_specs=[spec] * 5 + [pl.Bloc...  24.9 us
    ppermute x6, waiting for transfers between devices, turn_exchange(): lax.ppermute(x[d], axis, [(i, (i + d) % count) for i in range(count)])  15.8 us
    pallas_call x2, Pallas kernels, lower(): pl.pallas_call(bind(lower_kernel, slot_rows, cap), grid=(3,), in_specs=[p...  10.2 us
    pallas_call x1, Pallas kernels, on_device(): pl.pallas_call(bind(hidden_kernel, slot_rows, cap), grid=(tp_size,), in_s...  9 us
    pallas_call x1, Pallas kernels, run_mixer_final(): pl.pallas_call(mixer_final, grid_spec=pltpu.PrefetchScalarGridSpec(num_sc...  8.03 us
    ppermute x6, starting transfers between devices, turn_exchange(): lax.ppermute(x[d], axis, [(i, (i + d) % count) for i in range(count)])  7.95 us
  transfers between devices with their start and end apart: 12, of which 7 were waited for; matrix products, arithmetic and copies ran while one was open for 3% of the time, Pallas kernels for 22%

profile of v1, /device:TPU:33, one launch (start us, length us, event | category | flops | bytes accessed | tf_op | source)
XLA Modules:
  0.0 315.8 jit_solution(4952502289898665800)
XLA Ops:
  7.2 0.1 all-gather.5.cloned.1.call-start
  7.3 1.3 fusion.3
  8.6 0.4 reshape.60
  9.0 0.1 copy.25
  9.1 2.9 pad_maximum_fusion
  11.9 0.1 all-gather.5.cloned.1.call-update
  12.0 0.7 copy-done.9
  12.6 0.8 copy.23.x_ref
  13.5 24.9 %mixer_local.1 = (f32[512,512]{1,0:T(8,128)}, bf16[512,512]{1,0:T(8,128)(2,1)}, bf16[32,48,128]{2,1,0:T(8,128)(2,1)}) custom-call(bf16[512,512]{1,0:T(8,128)(2,1)} %q_ref.1, bf16[512,512]{1,0:T(8,128)(2,1)} %k_ref.1, bf16[512,512]{1,0:T(8,128)(2,1)} %v_ref.1, bf16[512,512]{1,0:T(8,128)(2,1)} %f_ref.1, bf16[512,512]{1,0:T(8,128)(2,1)} %a_ref.1, ...), custom_call_target="tpu_custom_call" | custom-call | flops 40000000000 | bytes 5000000 | tf_op jit(solution)/shard_map/mixer_local/pallas_call | solution.py:172
  38.3 25.5 %all-to-all-start.1 = ((bf16[32,48,128]{2,1,0:T(8,128)(2,1)}), bf16[32,48,128]{2,1,0:T(8,128)(2,1)S(1)}, u32[]{:S(2)}, u32[]{:S(2)}) async-start(bf16[32,48,128]{2,1,0:T(8,128)(2,1)} %get-tuple-element.11), calls=%async_computation.1 | async-start | bytes 786432 | tf_op jit(solution)/shard_map/all_to_all | solution.py:444
  63.8 0.7 copy.24.refs_2_
  64.6 3.7 %dispatch.1 = (bf16[1024,256]{1,0:T(8,128)(2,1)}, bf16[512,1536]{1,0:T(8,128)(2,1)}, s32[128,2]{1,0:T(8,128)}) custom-call(bf16[128,2048]{1,0:T(8,128)(2,1)} %refs_0_.1, f32[1,2048]{1,0:T(1,128)} %bitcast.67, s32[128,2]{1,0:T(8,128)} %copy.24.refs_2_), custom_call_target="tpu_custom_call" | custom-call | tf_op jit(solution)/shard_map/dispatch/pallas_call | solution.py:502
  68.2 23.1 %all-to-all-done.1.r_ref = bf16[32,48,128]{2,1,0:T(8,128)(2,1)S(1)} async-done(((bf16[32,48,128]{2,1,0:T(8,128)(2,1)}), bf16[32,48,128]{2,1,0:T(8,128)(2,1)S(1)}, u32[]{:S(2)}, u32[]{:S(2)}) %all-to-all-start.1) | async-done | bytes 393248 | tf_op jit(solution)/shard_map/all_to_all | solution.py:444
  91.4 4.5 %all-to-all-start = ((bf16[32,16,1536]{2,1,0:T(8,128)(2,1)}), bf16[32,16,1536]{2,1,0:T(8,128)(2,1)S(1)}, u32[]{:S(2)}, u32[]{:S(2)}) async-start(bf16[32,16,1536]{2,1,0:T(8,128)(2,1)} %bitcast.62), calls=%async_computation | async-start | bytes 3145728 | tf_op jit(solution)/shard_map/all_to_all | solution.py:444
  95.9 0.1 all-gather.7.cloned.1.call-start
  96.0 1.0 pad_maximum_fusion.1
  97.1 0.1 all-gather.7.cloned.1.call-update
  97.1 5.4 %chain.1 = bf16[32,16,128]{2,1,0:T(8,128)(2,1)} custom-call(bf16[32,48,128]{2,1,0:T(8,128)(2,1)} %copy-done.8), custom_call_target="tpu_custom_call" | custom-call | flops 3000000000 | bytes 600000 | tf_op jit(solution)/shard_map/chain/pallas_call | solution.py:210
  102.5 71.2 %all-to-all-done = bf16[32,16,1536]{2,1,0:T(8,128)(2,1)S(1)} async-done(((bf16[32,16,1536]{2,1,0:T(8,128)(2,1)}), bf16[32,16,1536]{2,1,0:T(8,128)(2,1)S(1)}, u32[]{:S(2)}, u32[]{:S(2)}) %all-to-all-start) | async-done | bytes 1572896 | tf_op jit(solution)/shard_map/all_to_all | solution.py:444
  173.8 1.2 copy-done
  174.9 9.0 %hidden.1.refs_0_ = bf16[512,1024]{1,0:T(8,128)(2,1)} custom-call(bf16[512,1536]{1,0:T(8,128)(2,1)} %bitcast.52, bf16[4,5120,256]{2,1,0:T(8,128)(2,1)} %bitcast.45, bf16[4,5120,256]{2,1,0:T(8,128)(2,1)} %bitcast.46), custom_call_target="tpu_custom_call" | custom-call | tf_op jit(solution)/shard_map/hidden/pallas_call | solution.py:535
  183.9 5.1 %lower.2 = bf16[512,896]{1,0:T(8,128)(2,1)} custom-call(bf16[512,1024]{1,0:T(8,128)(2,1)} %hidden.1.refs_0_, bf16[4,5120,256]{2,1,0:T(8,128)(2,1)} %bitcast.47, bf16[4,5120,256]{2,1,0:T(8,128)(2,1)} %bitcast.48, bf16[512,128]{1,0:T(8,128)(2,1)} %bitcast.66), custom_call_target="tpu_custom_call" | custom-call | tf_op jit(solution)/shard_map/lower/pallas_call | solution.py:552
  189.0 5.2 %all-to-all-start.2 = ((bf16[32,16,896]{2,1,0:T(8,128)(2,1)}), bf16[32,16,896]{2,1,0:T(8,128)(2,1)S(1)}, u32[]{:S(2)}, u32[]{:S(2)}) async-start(bf16[32,16,896]{2,1,0:T(8,128)(2,1)} %bitcast.55), calls=%async_computation.2 | async-start | bytes 1835008 | tf_op jit(solution)/shard_map/all_to_all | solution.py:444
  194.2 0.0 all-gather.7.cloned.1.call-done
  194.2 5.1 %lower.3 = bf16[512,768]{1,0:T(8,128)(2,1)} custom-call(bf16[512,1024]{1,0:T(8,128)(2,1)} %hidden.1.refs_0_, bf16[4,2048,256]{2,1,0:T(8,128)(2,1)} %bitcast.49, bf16[4,2048,256]{2,1,0:T(8,128)(2,1)} %bitcast.50), custom_call_target="tpu_custom_call" | custom-call | tf_op jit(solution)/shard_map/lower/pallas_call | solution.py:552
  199.3 45.0 %all-to-all-done.2 = bf16[32,16,896]{2,1,0:T(8,128)(2,1)S(1)} async-done(((bf16[32,16,896]{2,1,0:T(8,128)(2,1)}), bf16[32,16,896]{2,1,0:T(8,128)(2,1)S(1)}, u32[]{:S(2)}, u32[]{:S(2)}) %all-to-all-start.2) | async-done | bytes 917536 | tf_op jit(solution)/shard_map/all_to_all | solution.py:444
  244.2 5.0 %all-to-all-start.3 = ((bf16[32,16,768]{2,1,0:T(8,128)(2,1)}), bf16[32,16,768]{2,1,0:T(8,128)(2,1)S(1)}, u32[]{:S(2)}, u32[]{:S(2)}) async-start(bf16[32,16,768]{2,1,0:T(8,128)(2,1)} %bitcast.56), calls=%async_computation.3 | async-start | bytes 1572864 | tf_op jit(solution)/shard_map/all_to_all | solution.py:444
  249.3 5.7 %shared.1 = bf16[4,128,2048]{2,1,0:T(8,128)(2,1)} custom-call(s32[1]{0:T(128)} %bitcast.me_ref, bf16[4,2048,256]{2,1,0:T(8,128)(2,1)} %bitcast.51, bf16[2048,128]{1,0:T(8,128)(2,1)} %g_ref.3, bf16[2048,128]{1,0:T(8,128)(2,1)} %u_ref.1, bf16[128,2048]{1,0:T(8,128)(2,1)} %d_ref.1), custom_call_target="tpu_custom_call" | custom-call | tf_op jit(solution)/shard_map/shared/pallas_call | solution.py:578
  255.0 2.7 slice_bitcast_fusion
  257.7 1.4 collective-permute-start.3
  259.1 2.7 collective-permute-start.4
  261.8 1.0 collective-permute-start.5
  262.8 8.0 %mixer_final.1 = bf16[4,128,2048]{2,1,0:T(8,128)(2,1)} custom-call(s32[1]{0:T(128)} %bitcast.me_ref, f32[512,512]{1,0:T(8,128)} %get-tuple-element.8.o_ref, bf16[512,512]{1,0:T(8,128)(2,1)} %get-tuple-element.9.q2_ref, bf16[512,896]{1,0:T(8,128)(2,1)} %bitcast.53, bf16[512,512]{1,0:T(8,128)(2,1)} %g_ref.2, f32[1,512]{1,0:T(1,128)} %bitcast.70, ...), custom_call_target="tpu_custom_call" | custom-call | flops 6000000000 | bytes 8000000 | tf_op jit(solution)/shard_map/mixer_final/pallas_call | solution.py:257
  270.9 2.6 slice_bitcast_fusion.6
  273.4 0.5 collective-permute-start
  273.9 0.7 collective-permute-start.1
  274.6 0.0 collective-permute-done.3.refs_5_
  274.6 1.7 collective-permute-start.2
  276.3 0.7 copy.27.refs_3_
  277.0 7.1 %collective-permute-done.4.refs_6_ = bf16[128,2048]{1,0:T(8,128)(2,1)S(1)} collective-permute-done((bf16[128,2048]{1,0:T(8,128)(2,1)}, bf16[128,2048]{1,0:T(8,128)(2,1)S(1)}, u32[]{:S(2)}, u32[]{:S(2)}) %collective-permute-start.4) | collective-permute-done | bytes 524320 | tf_op jit(solution)/shard_map/ppermute | solution.py:439
  284.1 0.9 collective-permute-done.5.refs_7_
  285.0 8.8 %all-to-all-done.3 = bf16[32,16,768]{2,1,0:T(8,128)(2,1)S(1)} async-done(((bf16[32,16,768]{2,1,0:T(8,128)(2,1)}), bf16[32,16,768]{2,1,0:T(8,128)(2,1)S(1)}, u32[]{:S(2)}, u32[]{:S(2)}) %all-to-all-start.3) | async-done | bytes 786464 | tf_op jit(solution)/shard_map/all_to_all | solution.py:444
  293.8 0.9 copy-done.2
  294.7 4.1 %combine.1 = bf16[128,2048]{1,0:T(8,128)(2,1)} custom-call(bf16[512,896]{1,0:T(8,128)(2,1)} %bitcast.54, bf16[512,768]{1,0:T(8,128)(2,1)} %bitcast.57, s32[128,2]{1,0:T(8,128)} %get-tuple-element.13.refs_2_, f32[128,2]{1,0:T(8,128)} %copy.27.refs_3_, bf16[128,2048]{1,0:T(8,128)(2,1)} %get-tuple-element.17.refs_4_, bf16[128,2048]{1,0:T(8,128)(2,1)} %copy-done.4, ...), custom_call_target="tpu_custom_call" | custom-call | tf_op jit(solution)/shard_map/combine/pallas_call | solution.py:616
  298.8 0.0 collective-permute-done
  298.8 7.7 %collective-permute-done.1 = bf16[128,2048]{1,0:T(8,128)(2,1)S(1)} collective-permute-done((bf16[128,2048]{1,0:T(8,128)(2,1)}, bf16[128,2048]{1,0:T(8,128)(2,1)S(1)}, u32[]{:S(2)}, u32[]{:S(2)}) %collective-permute-start.1) | collective-permute-done | bytes 524320 | tf_op jit(solution)/shard_map/ppermute | solution.py:439
  306.5 0.0 collective-permute-done.2
  306.6 2.3 fusion.2
  (23 shorter events, 0.1 us)
Async XLA Ops:
  7.2 1.9 copy-start.3
  7.2 166.6 %all-gather.5.cloned.1.call-start = ((), (), s32[]{:S(2)}) async-start(), calls=%async_computation.4 | async-start | bytes 13107200 | tf_op jit(solution)/shard_map/all_gather | solution.py:490
  11.9 0.7 copy-start.9
  13.5 50.3 %copy-start.10 = (s32[128,2]{0,1:T(2,128)S(1)}, s32[128,2]{0,1:T(2,128)}, u32[]{:S(2)}) copy-start(s32[128,2]{0,1:T(2,128)} %param.34) | copy-start | bytes 3076
  38.3 53.0 %all-to-all-start.1 = ((bf16[32,48,128]{2,1,0:T(8,128)(2,1)}), bf16[32,48,128]{2,1,0:T(8,128)(2,1)S(1)}, u32[]{:S(2)}, u32[]{:S(2)}) async-start(bf16[32,48,128]{2,1,0:T(8,128)(2,1)} %get-tuple-element.11), calls=%async_computation.1 | async-start | bytes 786432 | tf_op jit(solution)/shard_map/all_to_all | solution.py:444
  68.2 27.8 %copy-start.7 = (bf16[1024,256]{1,0:T(8,128)(2,1)S(1)}, bf16[1024,256]{1,0:T(8,128)(2,1)}, u32[]{:S(2)}) copy-start(bf16[1024,256]{1,0:T(8,128)(2,1)} %get-tuple-element.12) | copy-start | bytes 1572868
  91.4 5.7 %copy-start.8 = (bf16[32,48,128]{2,1,0:T(8,128)(2,1)}, bf16[32,48,128]{2,1,0:T(8,128)(2,1)S(1)}, u32[]{:S(2)}) copy-start(bf16[32,48,128]{2,1,0:T(8,128)(2,1)S(1)} %all-to-all-done.1.r_ref) | copy-start | bytes 1179652
  91.4 82.4 %all-to-all-start = ((bf16[32,16,1536]{2,1,0:T(8,128)(2,1)}), bf16[32,16,1536]{2,1,0:T(8,128)(2,1)S(1)}, u32[]{:S(2)}, u32[]{:S(2)}) async-start(bf16[32,16,1536]{2,1,0:T(8,128)(2,1)} %bitcast.62), calls=%async_computation | async-start | bytes 3145728 | tf_op jit(solution)/shard_map/all_to_all | solution.py:444
  95.9 98.3 %all-gather.7.cloned.1.call-start = ((), (), s32[]{:S(2)}) async-start(), calls=%async_computation.5 | async-start | bytes 5242880 | tf_op jit(solution)/shard_map/all_gather | solution.py:513
  173.7 1.2 copy-start
  189.0 55.2 %all-to-all-start.2 = ((bf16[32,16,896]{2,1,0:T(8,128)(2,1)}), bf16[32,16,896]{2,1,0:T(8,128)(2,1)S(1)}, u32[]{:S(2)}, u32[]{:S(2)}) async-start(bf16[32,16,896]{2,1,0:T(8,128)(2,1)} %bitcast.55), calls=%async_computation.2 | async-start | bytes 1835008 | tf_op jit(solution)/shard_map/all_to_all | solution.py:444
  244.2 10.7 %copy-start.1 = (bf16[32,16,896]{2,1,0:T(8,128)(2,1)}, bf16[32,16,896]{2,1,0:T(8,128)(2,1)S(1)}, u32[]{:S(2)}) copy-start(bf16[32,16,896]{2,1,0:T(8,128)(2,1)S(1)} %all-to-all-done.2) | copy-start | bytes 2752516
  244.2 49.5 %all-to-all-start.3 = ((bf16[32,16,768]{2,1,0:T(8,128)(2,1)}), bf16[32,16,768]{2,1,0:T(8,128)(2,1)S(1)}, u32[]{:S(2)}, u32[]{:S(2)}) async-start(bf16[32,16,768]{2,1,0:T(8,128)(2,1)} %bitcast.56), calls=%async_computation.3 | async-start | bytes 1572864 | tf_op jit(solution)/shard_map/all_to_all | solution.py:444
  257.7 16.9 %collective-permute-start.3 = (bf16[128,2048]{1,0:T(8,128)(2,1)S(1)}, bf16[128,2048]{1,0:T(8,128)(2,1)S(1)}, u32[]{:S(2)}, u32[]{:S(2)}) collective-permute-start(bf16[128,2048]{1,0:T(8,128)(2,1)S(1)} %get-tuple-element.16), channel_id=1, source_target_pairs={{0,1},{1,2},{2,3},{3,0},{4,5},{5,6},{6,7},{7,4},{8,9},{9,10},{10,1... | collective-permute-start | bytes 1572872 | tf_op jit(solution)/shard_map/ppermute | solution.py:439
  259.1 25.0 %collective-permute-start.4 = (bf16[128,2048]{1,0:T(8,128)(2,1)}, bf16[128,2048]{1,0:T(8,128)(2,1)S(1)}, u32[]{:S(2)}, u32[]{:S(2)}) collective-permute-start(bf16[128,2048]{1,0:T(8,128)(2,1)} %get-tuple-element.15), channel_id=1, source_target_pairs={{0,2},{1,3},{2,0},{3,1},{4,6},{5,7},{6,4},{7,5},{8,10},{9,11},{10,... | collective-permute-start | bytes 1572872 | tf_op jit(solution)/shard_map/ppermute | solution.py:439
  261.8 23.2 %collective-permute-start.5 = (bf16[128,2048]{1,0:T(8,128)(2,1)}, bf16[128,2048]{1,0:T(8,128)(2,1)S(1)}, u32[]{:S(2)}, u32[]{:S(2)}) collective-permute-start(bf16[128,2048]{1,0:T(8,128)(2,1)} %get-tuple-element.14), channel_id=1, source_target_pairs={{0,3},{1,0},{2,1},{3,2},{4,7},{5,4},{6,5},{7,6},{8,11},{9,8},{10,9... | collective-permute-start | bytes 1572872 | tf_op jit(solution)/shard_map/ppermute | solution.py:439
  270.9 5.4 %copy-start.11 = (f32[128,2]{0,1:T(2,128)S(1)}, f32[128,2]{0,1:T(2,128)}, u32[]{:S(2)}) copy-start(f32[128,2]{0,1:T(2,128)} %param.35) | copy-start | bytes 3076
  273.4 25.4 %collective-permute-start = (bf16[128,2048]{1,0:T(8,128)(2,1)}, bf16[128,2048]{1,0:T(8,128)(2,1)S(1)}, u32[]{:S(2)}, u32[]{:S(2)}) collective-permute-start(bf16[128,2048]{1,0:T(8,128)(2,1)} %get-tuple-element.18), channel_id=1, source_target_pairs={{0,1},{1,2},{2,3},{3,0},{4,5},{5,6},{6,7},{7,4},{8,9},{9,10},{10,1... | collective-permute-start | bytes 1572872 | tf_op jit(solution)/shard_map/ppermute | solution.py:439
  273.9 32.7 %collective-permute-start.1 = (bf16[128,2048]{1,0:T(8,128)(2,1)}, bf16[128,2048]{1,0:T(8,128)(2,1)S(1)}, u32[]{:S(2)}, u32[]{:S(2)}) collective-permute-start(bf16[128,2048]{1,0:T(8,128)(2,1)} %get-tuple-element.20), channel_id=1, source_target_pairs={{0,2},{1,3},{2,0},{3,1},{4,6},{5,7},{6,4},{7,5},{8,10},{9,11},{10,... | collective-permute-start | bytes 1572872 | tf_op jit(solution)/shard_map/ppermute | solution.py:439
  274.6 19.2 %copy-start.4 = (bf16[128,2048]{1,0:T(8,128)(2,1)}, bf16[128,2048]{1,0:T(8,128)(2,1)S(1)}, u32[]{:S(2)}) copy-start(bf16[128,2048]{1,0:T(8,128)(2,1)S(1)} %collective-permute-done.3.refs_5_) | copy-start | bytes 1572868
  274.6 32.0 %collective-permute-start.2 = (bf16[128,2048]{1,0:T(8,128)(2,1)}, bf16[128,2048]{1,0:T(8,128)(2,1)}, u32[]{:S(2)}, u32[]{:S(2)}) collective-permute-start(bf16[128,2048]{1,0:T(8,128)(2,1)} %get-tuple-element.19), channel_id=1, source_target_pairs={{0,3},{1,0},{2,1},{3,2},{4,7},{5,4},{6,5},{7,6},{8,11},{9,8},{10,9... | collective-permute-start | bytes 1572872 | tf_op jit(solution)/shard_map/ppermute | solution.py:439
  284.1 9.7 %copy-start.5 = (bf16[128,2048]{1,0:T(8,128)(2,1)}, bf16[128,2048]{1,0:T(8,128)(2,1)S(1)}, u32[]{:S(2)}) copy-start(bf16[128,2048]{1,0:T(8,128)(2,1)S(1)} %collective-permute-done.4.refs_6_) | copy-start | bytes 1572868
  285.0 8.8 %copy-start.6 = (bf16[128,2048]{1,0:T(8,128)(2,1)}, bf16[128,2048]{1,0:T(8,128)(2,1)S(1)}, u32[]{:S(2)}) copy-start(bf16[128,2048]{1,0:T(8,128)(2,1)S(1)} %collective-permute-done.5.refs_7_) | copy-start | bytes 1572868
  293.8 0.9 copy-start.2
Sparse Core Ops, SparseCore 0:
  12.1 121.3 all-gather.4
  135.3 55.2 all-gather.6
